TPU v7x, 32 devices: a whole 2x2x4 slice. The times are simulated.
32 devices in a mesh: fs: 4 (over z), rep: 4 (over y, x), tp: 2 (over core).
Axes of the slice: x: 2, y: 2, z: 4, core: 2. Of those that a mesh axis runs over, the one named last changes fastest.
Arguments:
- normed_in: bfloat16 [24576, 2048], P(('fs', 'rep')), may hold values from -6 to 6
- cotan_rec: bfloat16 [24576, 2048], P(('fs', 'rep'), 'tp'), may hold values from -0.0390625 to 0.0390625
- cotan_gate: bfloat16 [24576, 2048], P(('fs', 'rep'), 'tp'), may hold values from -0.0390625 to 0.0390625
- factor_rec: bfloat16 [2048, 512], P('fs'), may hold values from -0.125 to 0.125
- factor_gate: bfloat16 [2048, 512], P('fs'), may hold values from -0.125 to 0.125
- first_rec: float32 [512, 2048], P('fs', 'tp'), may hold values from -6 to 6
- first_gate: float32 [512, 2048], P('fs', 'tp'), may hold values from -6 to 6
- second_rec: float32 [512, 2048], P('fs', 'tp'), may hold values from 0.25 to 4
- second_gate: float32 [512, 2048], P('fs', 'tp'), may hold values from 0.25 to 4
- master_rec: float32 [2048, 2048], P('fs', 'tp'), may hold values from -0.125 to 0.125
- master_gate: float32 [2048, 2048], P('fs', 'tp'), may hold values from -0.125 to 0.125
Outputs:
- update_rec: float32 [2048, 2048], P('fs', 'tp')
- update_gate: float32 [2048, 2048], P('fs', 'tp')
- new_first_rec: float32 [512, 2048], P('fs', 'tp')
- new_first_gate: float32 [512, 2048], P('fs', 'tp')
- new_second_rec: float32 [512, 2048], P('fs', 'tp')
- new_second_gate: float32 [512, 2048], P('fs', 'tp')
- copy_rec: bfloat16 [2048, 2048], P(None, 'tp')
- copy_gate: bfloat16 [2048, 2048], P(None, 'tp')
All inputs are finite; a program needn't handle non-finite values.
Results may differ from a plain program's by a relative error of at most 0.007.
Values may be sent and summed in bfloat16 or wider, within the bound.
A program may use at most 128 MiB of HBM per device.

v0:
```python
import jax
import jax.numpy as jnp
from jax import lax
from jax.sharding import PartitionSpec as P

DR = 2048
RANK = 512
beta_first = 0.8
beta_second = 0.9
scale_floor = 0.25
step_rate = 0.01


def split_product(projected, cotan):
    upper = projected.astype(jnp.bfloat16)
    lower = (projected - upper.astype(jnp.float32)).astype(jnp.bfloat16)
    dims = (((0,), (0,)), ((), ()))
    return lax.dot_general(
        upper, cotan, dims, preferred_element_type=jnp.float32
    ) + lax.dot_general(lower, cotan, dims, preferred_element_type=jnp.float32)


def moments(low, first, second):
    new_first = beta_first * first + (1.0 - beta_first) * low
    new_second = beta_second * second + (1.0 - beta_second) * low * low
    return (new_first, new_second, new_first / jnp.sqrt(new_second))


def body(
    normed_in,
    cotan_rec,
    cotan_gate,
    factor_rec,
    factor_gate,
    first_rec,
    first_gate,
    second_rec,
    second_gate,
    master_rec,
    master_gate,
):
    wide_rec = factor_rec.astype(jnp.float32)
    wide_gate = factor_gate.astype(jnp.float32)
    pieces = (
        lax.all_gather(factor_rec, "fs", axis=0, tiled=True),
        lax.all_gather(factor_gate, "fs", axis=0, tiled=True),
    )
    proj_rec = jnp.dot(normed_in, pieces[0], preferred_element_type=jnp.float32)
    proj_gate = jnp.dot(normed_in, pieces[1], preferred_element_type=jnp.float32)
    part_rec = split_product(proj_rec, cotan_rec)
    part_gate = split_product(proj_gate, cotan_gate)
    low_rec, low_gate = (
        lax.psum_scatter(
            part_rec.astype(jnp.bfloat16), "fs", scatter_dimension=0, tiled=True
        ).astype(jnp.float32),
        lax.psum_scatter(
            part_gate.astype(jnp.bfloat16), "fs", scatter_dimension=0, tiled=True
        ).astype(jnp.float32),
    )
    low_rec, low_gate = (
        lax.psum(low_rec.astype(jnp.bfloat16), "rep").astype(jnp.float32),
        lax.psum(low_gate.astype(jnp.bfloat16), "rep").astype(jnp.float32),
    )
    first_r, second_r, direc_rec = moments(low_rec, first_rec, second_rec)
    first_g, second_g, direc_gate = moments(low_gate, first_gate, second_gate)
    total_rec, total_gate = lax.psum(
        (jnp.sum(direc_rec * direc_rec), jnp.sum(direc_gate * direc_gate)), ("fs", "tp")
    )
    entries = float(RANK * DR)
    scale_rec = 1.0 / jnp.sqrt(total_rec / entries + scale_floor)
    scale_gate = 1.0 / jnp.sqrt(total_gate / entries + scale_floor)
    pieces = (
        lax.all_gather(direc_rec, "fs", axis=0, tiled=True),
        lax.all_gather(direc_gate, "fs", axis=0, tiled=True),
    )
    upd_rec = jnp.dot(wide_rec, pieces[0], precision=lax.Precision.HIGHEST)
    upd_gate = jnp.dot(wide_gate, pieces[1], precision=lax.Precision.HIGHEST)
    upd_rec = upd_rec * scale_rec
    upd_gate = upd_gate * scale_gate
    copy_rec = (master_rec - step_rate * upd_rec).astype(jnp.bfloat16)
    copy_gate = (master_gate - step_rate * upd_gate).astype(jnp.bfloat16)
    whole_rec, whole_gate = (
        lax.all_gather(copy_rec, "fs", axis=0, tiled=True),
        lax.all_gather(copy_gate, "fs", axis=0, tiled=True),
    )
    return (upd_rec, upd_gate, first_r, first_g, second_r, second_g, whole_rec, whole_gate)


def solution(mesh):
    return jax.shard_map(
        body,
        mesh=mesh,
        in_specs=(
            P(("fs", "rep"), None),
            P(("fs", "rep"), "tp"),
            P(("fs", "rep"), "tp"),
            P("fs", None),
            P("fs", None),
            P("fs", "tp"),
            P("fs", "tp"),
            P("fs", "tp"),
            P("fs", "tp"),
            P("fs", "tp"),
            P("fs", "tp"),
        ),
        out_specs=(
            P("fs", "tp"),
            P("fs", "tp"),
            P("fs", "tp"),
            P("fs", "tp"),
            P("fs", "tp"),
            P("fs", "tp"),
            P(None, "tp"),
            P(None, "tp"),
        ),
        check_vma=False,
    )
```

profile of v0, /device:TPU:0, one launch (start us, length us, event | category | flops | bytes accessed | tf_op | source)
XLA Modules:
  0.0 479.8 jit_solution(12746524796464819024)
XLA Ops:
  8.7 49.3 %all-gather.7.cloned.1.call-done = bf16[2048,512]{1,0:T(8,128)(2,1)} async-done(((bf16[512,512]{1,0:T(8,128)(2,1)}), bf16[2048,512]{1,0:T(8,128)(2,1)}) %all-gather.7.cloned.1.call-update) | async-done | bytes 2097168 | tf_op jit(solution)/shard_map/all_gather | solution.py:45
  58.0 6.1 %fusion.14 = f32[1536,512]{1,0:T(8,128)S(1)} fusion(bf16[1536,2048]{1,0:T(8,128)(2,1)} %param.11, bf16[2048,512]{1,0:T(8,128)(2,1)} %all-gather.7.cloned.1.call-done), kind=kOutput, calls=%fused_computation.26 | convolution fusion | flops 3221225472 | bytes 11534336 | tf_op jit(solution)/shard_map/dot_general | solution.py:48
  64.1 1.9 fusion
  66.0 2.9 add_convert_fusion.1
  69.0 35.1 %all-gather.11.cloned.1.call-done = bf16[2048,512]{1,0:T(8,128)(2,1)} async-done(((bf16[512,512]{1,0:T(8,128)(2,1)}), bf16[2048,512]{1,0:T(8,128)(2,1)}) %all-gather.11.cloned.1.call-update) | async-done | bytes 2097168 | tf_op jit(solution)/shard_map/all_gather | solution.py:46
  104.0 6.1 %fusion.15 = f32[1536,512]{1,0:T(8,128)S(1)} fusion(bf16[1536,2048]{1,0:T(8,128)(2,1)} %param.11, bf16[2048,512]{1,0:T(8,128)(2,1)} %all-gather.11.cloned.1.call-done), kind=kOutput, calls=%fused_computation.27 | convolution fusion | flops 3221225472 | bytes 11534336 | tf_op jit(solution)/shard_map/dot_general | solution.py:49
  110.2 1.9 fusion.1
  112.1 2.9 add_convert_fusion
  115.0 18.0 %reduce-scatter.3.cloned.1.call-done = bf16[128,1024]{1,0:T(8,128)(2,1)} async-done(((bf16[512,1024]{1,0:T(8,128)(2,1)}), bf16[128,1024]{1,0:T(8,128)(2,1)}) %reduce-scatter.3.cloned.1.call-update) | async-done | bytes 262160 | tf_op jit(solution)/shard_map/reduce_scatter | solution.py:53
  133.0 28.6 %reduce-scatter.5.cloned.1.call-done = bf16[128,1024]{1,0:T(8,128)(2,1)} async-done(((bf16[512,1024]{1,0:T(8,128)(2,1)}), bf16[128,1024]{1,0:T(8,128)(2,1)}) %reduce-scatter.5.cloned.1.call-update) | async-done | bytes 262160 | tf_op jit(solution)/shard_map/reduce_scatter | solution.py:56
  161.7 46.7 %all-reduce.4.cloned.1.call-done = (bf16[128,1024]{1,0:T(8,128)(2,1)}, bf16[128,1024]{1,0:T(8,128)(2,1)}) async-done(((bf16[128,1024]{1,0:T(8,128)(2,1)}, bf16[128,1024]{1,0:T(8,128)(2,1)}), (bf16[128,1024]{1,0:T(8,128)(2,1)}, bf16[128,1024]{1,0:T(8,128)(2,1)})) %all-reduce.4.cloned.1.call-update) | async-done | bytes 524304 | tf_op jit(solution)/shard_map/psum | solution.py:61
  208.4 3.2 multiply_reduce_fusion.1
  211.6 1.9 multiply_reduce_fusion
  215.5 17.6 %all-reduce = (f32[]{:T(128)}, f32[]{:T(128)}) all-reduce(f32[]{:T(128)} %get-tuple-element.24, f32[]{:T(128)} %get-tuple-element.20), channel_id=1, replica_groups=mesh['fs'=4,'rep'=4,'tp'=2] {'fs','tp'}, use_global_device_ids=true, to_apply=%region_3.0 | all-reduce | flops 2 | bytes 16 | tf_op jit(solution)/shard_map/psum | solution.py:66
  233.8 23.8 %all-gather.9.cloned.1.call-done = f32[512,1024]{1,0:T(8,128)} async-done(((f32[128,1024]{1,0:T(8,128)}), f32[512,1024]{1,0:T(8,128)}) %all-gather.9.cloned.1.call-update) | async-done | bytes 2097168 | tf_op jit(solution)/shard_map/all_gather | solution.py:73
  257.6 6.7 %subtract_convert_fusion.3 = (bf16[512,1024]{0,1:T(8,128)(2,1)}, f32[512,1024]{0,1:T(8,128)S(1)}) fusion(f32[512,1024]{0,1:T(8,128)} %copy.19, f32[]{:T(128)S(6)} %sqrt.13, f32[512,1024]{1,0:T(8,128)} %all-gather.9.cloned.1.call-done, bf16[512,512]{1,0:T(8,128)(2,1)S(1)} %copy-done.3), kind=kOutput, calls=%fused_computation.3 | convolution fusion | flops 3223322624 | bytes 7864324 | tf_op jit(solution)/shard_map/dot_general | solution.py:76
  264.4 3.0 copy.20
  268.1 36.1 %all-gather.13.cloned.1.call-done = f32[512,1024]{1,0:T(8,128)} async-done(((f32[128,1024]{1,0:T(8,128)}), f32[512,1024]{1,0:T(8,128)}) %all-gather.13.cloned.1.call-update) | async-done | bytes 2097168 | tf_op jit(solution)/shard_map/all_gather | solution.py:74
  304.2 7.5 %subtract_convert_fusion.2 = (bf16[512,1024]{0,1:T(8,128)(2,1)}, f32[512,1024]{0,1:T(8,128)}) fusion(f32[512,1024]{0,1:T(8,128)} %copy.20, f32[]{:T(128)S(6)} %sqrt.15, f32[512,1024]{1,0:T(8,128)} %all-gather.13.cloned.1.call-done, bf16[512,512]{1,0:T(8,128)(2,1)S(1)} %copy-done.4), kind=kOutput, calls=%fused_computation.2 | convolution fusion | flops 3223322624 | bytes 7864324 | tf_op jit(solution)/shard_map/dot_general | solution.py:77
  313.5 3.0 copy.22
  316.5 69.5 %all-gather.15.cloned.1.call-done = bf16[2048,1024]{0,1:T(8,128)(2,1)} async-done(((bf16[512,1024]{0,1:T(8,128)(2,1)}), bf16[2048,1024]{0,1:T(8,128)(2,1)}) %all-gather.15.cloned.1.call-update) | async-done | bytes 4194320 | tf_op jit(solution)/shard_map/all_gather | solution.py:83
  385.9 6.4 %copy.23 = bf16[2048,1024]{1,0:T(8,128)(2,1)} copy(bf16[2048,1024]{0,1:T(8,128)(2,1)} %all-gather.15.cloned.1.call-done) | data formatting | bytes 8388608
  392.3 74.4 %all-gather.17.cloned.1.call-done = bf16[2048,1024]{0,1:T(8,128)(2,1)} async-done(((bf16[512,1024]{0,1:T(8,128)(2,1)}), bf16[2048,1024]{0,1:T(8,128)(2,1)}) %all-gather.17.cloned.1.call-update) | async-done | bytes 4194320 | tf_op jit(solution)/shard_map/all_gather | solution.py:84
  466.8 6.5 %copy.24 = bf16[2048,1024]{1,0:T(8,128)(2,1)} copy(bf16[2048,1024]{0,1:T(8,128)(2,1)} %all-gather.17.cloned.1.call-done) | data formatting | bytes 8388608
  (38 shorter events, 5.6 us)
Async XLA Ops:
  7.2 56.9 %copy-start = (bf16[1536,1024]{1,0:T(8,128)(2,1)S(1)}, bf16[1536,1024]{1,0:T(8,128)(2,1)}, u32[]{:S(2)}) copy-start(bf16[1536,1024]{1,0:T(8,128)(2,1)} %param.12) | copy-start | bytes 9437188
  7.2 50.8 %all-gather.7.cloned.1.call-start = ((), (), s32[]{:S(2)}) async-start(), calls=%async_computation.2 | async-start | bytes 2621440 | tf_op jit(solution)/shard_map/all_gather | solution.py:45
  7.9 96.1 %all-gather.11.cloned.1.call-start = ((), (), s32[]{:S(2)}) async-start(), calls=%async_computation.5 | async-start | bytes 2621440 | tf_op jit(solution)/shard_map/all_gather | solution.py:46
  8.7 124.4 %reduce-scatter.3.cloned.1.call-start = ((), (), s32[]{:S(2)}) async-start(), calls=%async_computation.3 | async-start | bytes 1310720 | tf_op jit(solution)/shard_map/reduce_scatter | solution.py:53
  68.9 41.3 %copy-start.2 = (bf16[1536,1024]{1,0:T(8,128)(2,1)S(1)}, bf16[1536,1024]{1,0:T(8,128)(2,1)}, u32[]{:S(2)}) copy-start(bf16[1536,1024]{1,0:T(8,128)(2,1)} %param.13) | copy-start | bytes 9437188
  68.9 92.7 %reduce-scatter.5.cloned.1.call-start = ((), (), s32[]{:S(2)}) async-start(), calls=%async_computation.6 | async-start | bytes 1310720 | tf_op jit(solution)/shard_map/reduce_scatter | solution.py:56
  115.0 96.7 %copy-start.6 = (f32[128,1024]{1,0:T(8,128)S(1)}, f32[128,1024]{1,0:T(8,128)}, u32[]{:S(2)}) copy-start(f32[128,1024]{1,0:T(8,128)} %param.19) | copy-start | bytes 1572868
  115.0 96.6 %copy-start.7 = (f32[128,1024]{1,0:T(8,128)S(1)}, f32[128,1024]{1,0:T(8,128)}, u32[]{:S(2)}) copy-start(f32[128,1024]{1,0:T(8,128)} %param.17) | copy-start | bytes 1572868
  115.0 93.4 %all-reduce.4.cloned.1.call-start = ((), (), s32[]{:S(2)}) async-start(), calls=%async_computation.10 | async-start | bytes 1048576 | tf_op jit(solution)/shard_map/psum | solution.py:61
  161.6 96.0 %all-gather.9.cloned.1.call-start = ((), (), s32[]{:S(2)}) async-start(), calls=%async_computation.4 | async-start | bytes 2621440 | tf_op jit(solution)/shard_map/all_gather | solution.py:73
  208.4 3.3 copy-start.8
  211.5 2.2 copy-start.5
  211.6 92.6 %all-gather.13.cloned.1.call-start = ((), (), s32[]{:S(2)}) async-start(), calls=%async_computation.7 | async-start | bytes 2621440 | tf_op jit(solution)/shard_map/all_gather | solution.py:74
  213.6 44.1 %copy-start.3 = (bf16[512,512]{1,0:T(8,128)(2,1)S(1)}, bf16[512,512]{1,0:T(8,128)(2,1)}, u32[]{:S(2)}) copy-start(bf16[512,512]{1,0:T(8,128)(2,1)} %param.14) | copy-start | bytes 1572868
  213.6 172.4 %all-gather.15.cloned.1.call-start = ((), (), s32[]{:S(2)}) async-start(), calls=%async_computation.8 | async-start | bytes 5242880 | tf_op jit(solution)/shard_map/all_gather | solution.py:83
  264.3 39.9 %copy-start.4 = (bf16[512,512]{1,0:T(8,128)(2,1)S(1)}, bf16[512,512]{1,0:T(8,128)(2,1)}, u32[]{:S(2)}) copy-start(bf16[512,512]{1,0:T(8,128)(2,1)} %param.15) | copy-start | bytes 1572868
  264.3 202.4 %all-gather.17.cloned.1.call-start = ((), (), s32[]{:S(2)}) async-start(), calls=%async_computation.9 | async-start | bytes 5242880 | tf_op jit(solution)/shard_map/all_gather | solution.py:84
  466.8 6.5 %copy-start.1 = (bf16[1536,1024]{1,0:T(8,128)(2,1)S(1)}, bf16[1536,1024]{1,0:T(8,128)(2,1)}, u32[]{:S(2)}) copy-start(bf16[1536,1024]{1,0:T(8,128)(2,1)} %param.12) | copy-start | bytes 9437188
Sparse Core Ops, SparseCore 0:
  9.6 48.3 all-gather.6
  59.5 44.4 all-gather.10
  106.9 26.0 reduce-scatter.2
  135.7 25.7 reduce-scatter.4
  164.4 43.9 all-reduce.3
  211.7 45.8 all-gather.8
  259.8 44.4 all-gather.12
  306.3 79.5 all-gather.14
  387.5 79.2 all-gather.16
where the time goes:
time: 480 us
  waiting for transfers between devices  383 us (80%)
  matrix products  35.9 us (7%)
  local copies, waits for them, and re-layouts  22.7 us (5%)
  blocking collectives  17.6 us (4%)
  between operations  15.3 us (3%)
  other arithmetic  5.05 us (1%)
    all_gather x1, waiting for transfers between devices, body(): lax.all_gather(copy_gate, 'fs', axis=0, tiled=True)  74.4 us
    all_gather x1, waiting for transfers between devices, body(): lax.all_gather(copy_rec, 'fs', axis=0, tiled=True)  69.5 us
    all_gather x1, waiting for transfers between devices, body(): lax.all_gather(factor_rec, 'fs', axis=0, tiled=True)  49.3 us
    psum x1, waiting for transfers between devices, body(): lax.psum(low_rec.astype(jnp.bfloat16), 'rep').astype(jnp.float32)  46.7 us
    all_gather x1, waiting for transfers between devices, body(): lax.all_gather(direc_gate, 'fs', axis=0, tiled=True)  36.1 us
    all_gather x1, waiting for transfers between devices, body(): lax.all_gather(factor_gate, 'fs', axis=0, tiled=True)  35.1 us
    reduce_scatter x1, waiting for transfers between devices, body(): lax.psum_scatter(part_gate.astype(jnp.bfloat16), 'fs', scatter_dimension=...  28.6 us
    all_gather x1, waiting for transfers between devices, body(): lax.all_gather(direc_rec, 'fs', axis=0, tiled=True)  23.8 us
  transfers between devices with their start and end apart: 9, of which 9 were waited for; matrix products, arithmetic and copies ran while one was open for 11% of the time, Pallas kernels for 0%

commit v1 on v0

--- a/solution.py
+++ b/solution.py
@@ -58,7 +58,7 @@
         ).astype(jnp.float32),
     )
     low_rec, low_gate = (
-        lax.psum(low_rec.astype(jnp.bfloat16), "rep").astype(jnp.float32),
+        jnp.sum(lax.all_gather(low_rec.astype(jnp.bfloat16), "rep"), axis=0).astype(jnp.float32),
         lax.psum(low_gate.astype(jnp.bfloat16), "rep").astype(jnp.float32),
     )
     first_r, second_r, direc_rec = moments(low_rec, first_rec, second_rec)

time: 480 us -> 505 us (1.052)
  waiting for transfers between devices: 383 us -> 404 us
    all_gather x0 -> x1, waiting for transfers between devices: none -> 25.1 us  [body(): lax.all_gather(low_rec.astype(jnp.bfloat16), 'rep')]
    all_gather x1, waiting for transfers between devices: 35.1 us -> 49.3 us  [body(): lax.all_gather(factor_gate, 'fs', axis=0, tiled=True)]
    all_gather x1, waiting for transfers between devices: 49.3 us -> 35.1 us  [body(): lax.all_gather(factor_rec, 'fs', axis=0, tiled=True)]
    all_gather x1, waiting for transfers between devices: 36.1 us -> 23 us  [body(): lax.all_gather(direc_gate, 'fs', axis=0, tiled=True)]
    all_gather x1, waiting for transfers between devices: 23.8 us -> 36 us  [body(): lax.all_gather(direc_rec, 'fs', axis=0, tiled=True)]
    reduce_scatter x1, waiting for transfers between devices: 28.6 us -> 18 us  [body(): lax.psum_scatter(part_gate.astype(jnp.bfloat16), 'fs', scatter_dimension=...]
    reduce_scatter x1, waiting for transfers between devices: 18 us -> 28.5 us  [body(): lax.psum_scatter(part_rec.astype(jnp.bfloat16), 'fs', scatter_dimension=0...]
    all_gather x1, waiting for transfers between devices: 74.4 us -> 68.9 us  [body(): lax.all_gather(copy_gate, 'fs', axis=0, tiled=True)]
  transfers between devices with their start and end apart: 9 -> 10, of which waited for: 9 -> 10; matrix products, arithmetic and copies ran while one was open for 11% -> 12% of each run, Pallas kernels for 0% -> 0%
where the time goes in v1:
time: 505 us
  waiting for transfers between devices  404 us (80%)
  matrix products  35.9 us (7%)
  local copies, waits for them, and re-layouts  22.7 us (4%)
  blocking collectives  18.1 us (4%)
  between operations  15.6 us (3%)
  other arithmetic  7.57 us (1%)
    all_gather x1, waiting for transfers between devices, body(): lax.all_gather(copy_rec, 'fs', axis=0, tiled=True)  74.9 us
    all_gather x1, waiting for transfers between devices, body(): lax.all_gather(copy_gate, 'fs', axis=0, tiled=True)  68.9 us
    all_gather x1, waiting for transfers between devices, body(): lax.all_gather(factor_gate, 'fs', axis=0, tiled=True)  49.3 us
    psum x1, waiting for transfers between devices, body(): lax.psum(low_gate.astype(jnp.bfloat16), 'rep').astype(jnp.float32)  44.3 us
    all_gather x1, waiting for transfers between devices, body(): lax.all_gather(direc_rec, 'fs', axis=0, tiled=True)  36 us
    all_gather x1, waiting for transfers between devices, body(): lax.all_gather(factor_rec, 'fs', axis=0, tiled=True)  35.1 us
    reduce_scatter x1, waiting for transfers between devices, body(): lax.psum_scatter(part_rec.astype(jnp.bfloat16), 'fs', scatter_dimension=0...  28.5 us
    all_gather x1, waiting for transfers between devices, body(): lax.all_gather(low_rec.astype(jnp.bfloat16), 'rep')  25.1 us
  transfers between devices with their start and end apart: 10, of which 10 were waited for; matrix products, arithmetic and copies ran while one was open for 12% of the time, Pallas kernels for 0%

profile of v1, /device:TPU:0, one launch (start us, length us, event | category | flops | bytes accessed | tf_op | source)
XLA Modules:
  0.0 504.6 jit_solution(17767868257868395551)
XLA Ops:
  8.7 49.3 %all-gather.13.cloned.1.call-done = bf16[2048,512]{1,0:T(8,128)(2,1)} async-done(((bf16[512,512]{1,0:T(8,128)(2,1)}), bf16[2048,512]{1,0:T(8,128)(2,1)}) %all-gather.13.cloned.1.call-update) | async-done | bytes 2097168 | tf_op jit(solution)/shard_map/all_gather | solution.py:46
  58.0 6.1 %fusion.15 = f32[1536,512]{1,0:T(8,128)S(1)} fusion(bf16[1536,2048]{1,0:T(8,128)(2,1)} %param.11, bf16[2048,512]{1,0:T(8,128)(2,1)} %all-gather.13.cloned.1.call-done), kind=kOutput, calls=%fused_computation.27 | convolution fusion | flops 3221225472 | bytes 11534336 | tf_op jit(solution)/shard_map/dot_general | solution.py:49
  64.1 1.9 fusion.1
  66.0 2.9 add_convert_fusion
  69.0 35.1 %all-gather.9.cloned.1.call-done = bf16[2048,512]{1,0:T(8,128)(2,1)} async-done(((bf16[512,512]{1,0:T(8,128)(2,1)}), bf16[2048,512]{1,0:T(8,128)(2,1)}) %all-gather.9.cloned.1.call-update) | async-done | bytes 2097168 | tf_op jit(solution)/shard_map/all_gather | solution.py:45
  104.0 6.1 %fusion.14 = f32[1536,512]{1,0:T(8,128)S(1)} fusion(bf16[1536,2048]{1,0:T(8,128)(2,1)} %param.11, bf16[2048,512]{1,0:T(8,128)(2,1)} %all-gather.9.cloned.1.call-done), kind=kOutput, calls=%fused_computation.26 | convolution fusion | flops 3221225472 | bytes 11534336 | tf_op jit(solution)/shard_map/dot_general | solution.py:48
  112.1 2.9 add_convert_fusion.1
  115.0 18.0 %reduce-scatter.5.cloned.1.call-done = bf16[128,1024]{1,0:T(8,128)(2,1)} async-done(((bf16[512,1024]{1,0:T(8,128)(2,1)}), bf16[128,1024]{1,0:T(8,128)(2,1)}) %reduce-scatter.5.cloned.1.call-update) | async-done | bytes 262160 | tf_op jit(solution)/shard_map/reduce_scatter | solution.py:56
  133.1 28.5 %reduce-scatter.3.cloned.1.call-done = bf16[128,1024]{1,0:T(8,128)(2,1)} async-done(((bf16[512,1024]{1,0:T(8,128)(2,1)}), bf16[128,1024]{1,0:T(8,128)(2,1)}) %reduce-scatter.3.cloned.1.call-update) | async-done | bytes 262160 | tf_op jit(solution)/shard_map/reduce_scatter | solution.py:53
  161.7 44.3 %all-reduce.3.cloned.1.call-done = bf16[128,1024]{1,0:T(8,128)(2,1)} async-done(((bf16[128,1024]{1,0:T(8,128)(2,1)}), bf16[128,1024]{1,0:T(8,128)(2,1)}) %all-reduce.3.cloned.1.call-update) | async-done | bytes 262160 | tf_op jit(solution)/shard_map/psum | solution.py:62
  206.0 3.1 multiply_reduce_fusion
  209.1 25.1 %all-gather.21.cloned.1.call-done = bf16[512,1024]{1,0:T(8,128)(2,1)} async-done(((bf16[128,1024]{1,0:T(8,128)(2,1)}), bf16[512,1024]{1,0:T(8,128)(2,1)}) %all-gather.21.cloned.1.call-update) | async-done | bytes 1048592 | tf_op jit(solution)/shard_map/all_gather | solution.py:61
  235.8 2.9 multiply_reduce_fusion.1
  240.6 18.1 %all-reduce = (f32[]{:T(128)}, f32[]{:T(128)}) all-reduce(f32[]{:T(128)} %get-tuple-element.22, f32[]{:T(128)} %get-tuple-element.18), channel_id=1, replica_groups=mesh['fs'=4,'rep'=4,'tp'=2] {'fs','tp'}, use_global_device_ids=true, to_apply=%region_3.0 | all-reduce | flops 2 | bytes 16 | tf_op jit(solution)/shard_map/psum | solution.py:66
  259.3 23.0 %all-gather.15.cloned.1.call-done = f32[512,1024]{1,0:T(8,128)} async-done(((f32[128,1024]{1,0:T(8,128)}), f32[512,1024]{1,0:T(8,128)}) %all-gather.15.cloned.1.call-update) | async-done | bytes 2097168 | tf_op jit(solution)/shard_map/all_gather | solution.py:74
  282.2 6.8 %subtract_convert_fusion.2 = (bf16[512,1024]{0,1:T(8,128)(2,1)}, f32[512,1024]{0,1:T(8,128)S(1)}) fusion(f32[512,1024]{0,1:T(8,128)} %copy.20, f32[]{:T(128)S(6)} %sqrt.15, f32[512,1024]{1,0:T(8,128)} %all-gather.15.cloned.1.call-done, bf16[512,512]{1,0:T(8,128)(2,1)S(1)} %copy-done.3), kind=kOutput, calls=%fused_computation.2 | convolution fusion | flops 3223322624 | bytes 7864324 | tf_op jit(solution)/shard_map/dot_general | solution.py:77
  289.1 3.0 copy.19
  292.8 36.0 %all-gather.11.cloned.1.call-done = f32[512,1024]{1,0:T(8,128)} async-done(((f32[128,1024]{1,0:T(8,128)}), f32[512,1024]{1,0:T(8,128)}) %all-gather.11.cloned.1.call-update) | async-done | bytes 2097168 | tf_op jit(solution)/shard_map/all_gather | solution.py:73
  328.8 7.3 %subtract_convert_fusion.3 = (bf16[512,1024]{0,1:T(8,128)(2,1)}, f32[512,1024]{0,1:T(8,128)}) fusion(f32[512,1024]{0,1:T(8,128)} %copy.19, f32[]{:T(128)S(6)} %sqrt.13, f32[512,1024]{1,0:T(8,128)} %all-gather.11.cloned.1.call-done, bf16[512,512]{1,0:T(8,128)(2,1)S(1)} %copy-done.4), kind=kOutput, calls=%fused_computation.3 | convolution fusion | flops 3223322624 | bytes 7864324 | tf_op jit(solution)/shard_map/dot_general | solution.py:76
  338.0 3.0 copy.21
  341.1 68.9 %all-gather.19.cloned.1.call-done = bf16[2048,1024]{0,1:T(8,128)(2,1)} async-done(((bf16[512,1024]{0,1:T(8,128)(2,1)}), bf16[2048,1024]{0,1:T(8,128)(2,1)}) %all-gather.19.cloned.1.call-update) | async-done | bytes 4194320 | tf_op jit(solution)/shard_map/all_gather | solution.py:84
  410.0 6.4 %copy.24 = bf16[2048,1024]{1,0:T(8,128)(2,1)} copy(bf16[2048,1024]{0,1:T(8,128)(2,1)} %all-gather.19.cloned.1.call-done) | data formatting | bytes 8388608
  416.4 74.9 %all-gather.17.cloned.1.call-done = bf16[2048,1024]{0,1:T(8,128)(2,1)} async-done(((bf16[512,1024]{0,1:T(8,128)(2,1)}), bf16[2048,1024]{0,1:T(8,128)(2,1)}) %all-gather.17.cloned.1.call-update) | async-done | bytes 4194320 | tf_op jit(solution)/shard_map/all_gather | solution.py:83
  491.2 6.5 %copy.23 = bf16[2048,1024]{1,0:T(8,128)(2,1)} copy(bf16[2048,1024]{0,1:T(8,128)(2,1)} %all-gather.17.cloned.1.call-done) | data formatting | bytes 8388608
  (38 shorter events, 9.1 us)
Async XLA Ops:
  7.2 56.9 %copy-start = (bf16[1536,1024]{1,0:T(8,128)(2,1)S(1)}, bf16[1536,1024]{1,0:T(8,128)(2,1)}, u32[]{:S(2)}) copy-start(bf16[1536,1024]{1,0:T(8,128)(2,1)} %param.13) | copy-start | bytes 9437188
  7.2 50.8 %all-gather.13.cloned.1.call-start = ((), (), s32[]{:S(2)}) async-start(), calls=%async_computation.5 | async-start | bytes 2621440 | tf_op jit(solution)/shard_map/all_gather | solution.py:46
  7.9 96.1 %all-gather.9.cloned.1.call-start = ((), (), s32[]{:S(2)}) async-start(), calls=%async_computation.2 | async-start | bytes 2621440 | tf_op jit(solution)/shard_map/all_gather | solution.py:45
  8.7 124.4 %reduce-scatter.5.cloned.1.call-start = ((), (), s32[]{:S(2)}) async-start(), calls=%async_computation.6 | async-start | bytes 1310720 | tf_op jit(solution)/shard_map/reduce_scatter | solution.py:56
  68.9 41.3 %copy-start.2 = (bf16[1536,1024]{1,0:T(8,128)(2,1)S(1)}, bf16[1536,1024]{1,0:T(8,128)(2,1)}, u32[]{:S(2)}) copy-start(bf16[1536,1024]{1,0:T(8,128)(2,1)} %param.12) | copy-start | bytes 9437188
  68.9 92.7 %reduce-scatter.3.cloned.1.call-start = ((), (), s32[]{:S(2)}) async-start(), calls=%async_computation.3 | async-start | bytes 1310720 | tf_op jit(solution)/shard_map/reduce_scatter | solution.py:53
  115.0 91.0 %all-reduce.3.cloned.1.call-start = ((), (), s32[]{:S(2)}) async-start(), calls=%async_computation.7 | async-start | bytes 524288 | tf_op jit(solution)/shard_map/psum | solution.py:62
  133.0 101.1 %all-gather.21.cloned.1.call-start = ((), (), s32[]{:S(2)}) async-start(), calls=%async_computation.11 | async-start | bytes 1310720 | tf_op jit(solution)/shard_map/all_gather | solution.py:61
  161.6 74.2 %copy-start.6 = (f32[128,1024]{1,0:T(8,128)S(1)}, f32[128,1024]{1,0:T(8,128)}, u32[]{:S(2)}) copy-start(f32[128,1024]{1,0:T(8,128)} %param.18) | copy-start | bytes 1572868
  161.6 120.6 %all-gather.15.cloned.1.call-start = ((), (), s32[]{:S(2)}) async-start(), calls=%async_computation.8 | async-start | bytes 2621440 | tf_op jit(solution)/shard_map/all_gather | solution.py:74
  209.1 119.8 %all-gather.11.cloned.1.call-start = ((), (), s32[]{:S(2)}) async-start(), calls=%async_computation.4 | async-start | bytes 2621440 | tf_op jit(solution)/shard_map/all_gather | solution.py:73
  234.2 4.6 copy-start.5
  238.7 43.5 %copy-start.3 = (bf16[512,512]{1,0:T(8,128)(2,1)S(1)}, bf16[512,512]{1,0:T(8,128)(2,1)}, u32[]{:S(2)}) copy-start(bf16[512,512]{1,0:T(8,128)(2,1)} %param.15) | copy-start | bytes 1572868
  238.7 171.3 %all-gather.19.cloned.1.call-start = ((), (), s32[]{:S(2)}) async-start(), calls=%async_computation.10 | async-start | bytes 5242880 | tf_op jit(solution)/shard_map/all_gather | solution.py:84
  289.0 39.8 %copy-start.4 = (bf16[512,512]{1,0:T(8,128)(2,1)S(1)}, bf16[512,512]{1,0:T(8,128)(2,1)}, u32[]{:S(2)}) copy-start(bf16[512,512]{1,0:T(8,128)(2,1)} %param.14) | copy-start | bytes 1572868
  289.0 202.2 %all-gather.17.cloned.1.call-start = ((), (), s32[]{:S(2)}) async-start(), calls=%async_computation.9 | async-start | bytes 5242880 | tf_op jit(solution)/shard_map/all_gather | solution.py:83
  491.2 6.5 %copy-start.1 = (bf16[1536,1024]{1,0:T(8,128)(2,1)S(1)}, bf16[1536,1024]{1,0:T(8,128)(2,1)}, u32[]{:S(2)}) copy-start(bf16[1536,1024]{1,0:T(8,128)(2,1)} %param.13) | copy-start | bytes 9437188
Sparse Core Ops, SparseCore 0:
  9.6 48.3 all-gather.12
  59.5 44.4 all-gather.8
  106.9 26.0 reduce-scatter.4
  135.7 25.7 reduce-scatter.2
  164.4 41.5 all-reduce.2
  207.7 26.4 all-gather.20
  236.3 45.8 all-gather.14
  284.4 44.4 all-gather.10
  330.4 79.5 all-gather.18
  412.0 79.2 all-gather.16
